TPU v7x, 32 devices: a whole 2x2x4 slice. The times are simulated.
32 devices in a mesh: rep: 2 (over x), fs: 4 (over z), tp: 4 (over y, core).
Axes of the slice: x: 2, y: 2, z: 4, core: 2. Of those that a mesh axis runs over, the one named last changes fastest.
Arguments:
- tokens: bfloat16 [4096, 2048], P(('rep', 'fs', 'tp')), may hold values from -6 to 6
- norm_gain: float32 [2048], replicated, may hold values from 0.1 to 1.9
- gate_weight: float32 [2048, 5632], P('fs', 'tp'), may hold values from -0.125 to 0.125
- gate_scale: float32 [5632], P('tp'), may hold values from 0.5 to 2
- up_weight: float32 [2048, 5632], P('fs', 'tp'), may hold values from -0.125 to 0.125
- up_scale: float32 [5632], P('tp'), may hold values from 0.5 to 2
- down_weight: float32 [5632, 2048], P('tp', 'fs'), may hold values from -0.078125 to 0.078125
- down_scale: float32 [2048], P('fs'), may hold values from 0.5 to 2
Outputs:
- mixed: bfloat16 [4096, 2048], P(('rep', 'fs', 'tp'))
All inputs are finite; a program needn't handle non-finite values.
Results may differ from a plain program's by a relative error of at most 0.014.
Values may be sent and summed in bfloat16 or wider, within the bound.
A program may use at most 64 MiB of HBM per device.

v0:
```python
import jax
import jax.numpy as jnp
from jax import lax
from jax.sharding import PartitionSpec as P


def shards(
    tokens, norm_gain, gate_weight, gate_scale, up_weight, up_scale, down_weight, down_scale
):
    n_rep = lax.axis_size("rep")
    rep = lax.axis_index("rep")
    width = gate_weight.shape[1] // n_rep
    start = rep * width

    def part(array, axis):
        return lax.dynamic_slice_in_dim(array, start, width, axis)

    flat = tokens.astype(jnp.float32)
    mean_square = jnp.mean(flat * flat, axis=-1, keepdims=True)
    inverse = lax.rsqrt(mean_square + 1e-06)
    normed = (flat * inverse * norm_gain).astype(jnp.bfloat16)
    group = lax.all_gather(normed, ("rep", "tp"), axis=0, tiled=True)
    gate_low = part(gate_weight, 1).astype(jnp.bfloat16)
    up_low = part(up_weight, 1).astype(jnp.bfloat16)
    down_low = part(down_weight, 0).astype(jnp.bfloat16)
    gate = jnp.dot(
        group,
        lax.all_gather(gate_low, "fs", axis=0, tiled=True),
        preferred_element_type=jnp.float32,
    )
    up = jnp.dot(
        group, lax.all_gather(up_low, "fs", axis=0, tiled=True), preferred_element_type=jnp.float32
    )
    down_full = lax.all_gather(down_low, "fs", axis=1, tiled=True)
    gate = gate * part(gate_scale, 0)
    up = up * part(up_scale, 0)
    hidden = (jax.nn.silu(gate) * up).astype(jnp.bfloat16)
    scales = lax.all_gather(down_scale, "fs", axis=0, tiled=True)
    total = lax.psum_scatter(
        jnp.dot(hidden, down_full, preferred_element_type=jnp.float32).astype(jnp.bfloat16),
        ("rep", "tp"),
        scatter_dimension=0,
        tiled=True,
    ).astype(jnp.float32)
    return (total * scales).astype(jnp.bfloat16)


def solution(mesh):
    in_specs = (
        P(("rep", "fs", "tp"), None),
        P(),
        P("fs", "tp"),
        P("tp"),
        P("fs", "tp"),
        P("tp"),
        P("tp", "fs"),
        P("fs"),
    )
    out_specs = P(("rep", "fs", "tp"), None)
    return jax.shard_map(shards, mesh=mesh, in_specs=in_specs, out_specs=out_specs, check_vma=False)
```

profile of v0, /device:TPU:0, one launch (start us, length us, event | category | flops | bytes accessed | tf_op | source)
XLA Modules:
  0.0 308.1 jit_solution(6207909742359432319)
XLA Ops:
  6.5 0.0 copy-start
  6.5 0.0 copy-start.1
  6.5 0.0 copy-start.2
  6.5 0.0 all-gather.8.cloned.1.call-start
  6.6 1.8 copy-done
  8.4 1.2 dynamic-slice_convert_fusion.1
  9.6 0.0 all-gather.8.cloned.1.call-update
  9.6 0.0 all-gather.6.cloned.1.call-start
  9.7 1.2 fusion
  10.9 0.0 copy-done.1
  10.9 0.0 copy-done.2
  10.9 0.0 copy-start.4
  10.9 0.0 copy-start.5
  10.9 1.0 fusion.2
  11.9 0.0 all-gather.6.cloned.1.call-update
  11.9 0.0 all-gather.10.cloned.1.call-start
  12.0 2.7 dynamic-slice_convert_fusion
  14.7 0.0 all-gather.10.cloned.1.call-update
  14.8 0.0 all-gather.12.cloned.1.call-start
  14.8 2.3 dynamic-slice_convert_fusion.2
  17.1 0.0 all-gather.12.cloned.1.call-update
  17.2 0.0 reduce-scatter.2.cloned.1.call-start
  17.2 0.0 copy-done.4
  17.2 0.1 dynamic_slice.16
  17.3 0.0 copy-done.5
  17.3 0.1 dynamic_slice.18
  17.4 58.6 %all-gather.8.cloned.1.call-done = bf16[2048,704]{1,0:T(8,128)(2,1)} async-done(((bf16[512,704]{1,0:T(8,128)(2,1)}), bf16[2048,704]{1,0:T(8,128)(2,1)}) %all-gather.8.cloned.1.call-update) | async-done | bytes 2883600 | tf_op jit(solution)/shard_map/all_gather | solution.py:28
  75.9 37.1 %all-gather.6.cloned.1.call-done = bf16[1024,2048]{1,0:T(8,128)(2,1)} async-done(((bf16[128,2048]{1,0:T(8,128)(2,1)}), bf16[1024,2048]{1,0:T(8,128)(2,1)}) %all-gather.6.cloned.1.call-update) | async-done | bytes 4194320 | tf_op jit(solution)/shard_map/all_gather | solution.py:22
  113.1 7.9 %fusion.4 = f32[1024,704]{0,1:T(8,128)} fusion(bf16[1024,2048]{1,0:T(8,128)(2,1)} %all-gather.6.cloned.1.call-done, bf16[2048,704]{1,0:T(8,128)(2,1)} %all-gather.8.cloned.1.call-done), kind=kOutput, calls=%fused_computation.13 | convolution fusion | flops 2952790016 | bytes 9961472 | tf_op jit(solution)/shard_map/dot_general | solution.py:26
  121.0 57.1 %all-gather.10.cloned.1.call-done = bf16[2048,704]{1,0:T(8,128)(2,1)} async-done(((bf16[512,704]{1,0:T(8,128)(2,1)}), bf16[2048,704]{1,0:T(8,128)(2,1)}) %all-gather.10.cloned.1.call-update) | async-done | bytes 2883600 | tf_op jit(solution)/shard_map/all_gather | solution.py:32
  178.1 59.2 %all-gather.12.cloned.1.call-done = bf16[704,2048]{1,0:T(8,128)(2,1)} async-done(((bf16[704,512]{1,0:T(8,128)(2,1)}), bf16[704,2048]{1,0:T(8,128)(2,1)}) %all-gather.12.cloned.1.call-update) | async-done | bytes 2883600 | tf_op jit(solution)/shard_map/all_gather | solution.py:34
  237.3 12.3 %convolution_convert_fusion = bf16[1024,2048]{1,0:T(8,128)(2,1)} fusion(bf16[704,2048]{1,0:T(8,128)(2,1)} %all-gather.12.cloned.1.call-done, f32[1024,704]{0,1:T(8,128)} %fusion.4, bf16[1024,2048]{1,0:T(8,128)(2,1)} %all-gather.6.cloned.1.call-done, bf16[2048,704]{1,0:T(8,128)(2,1)} %all-gather.10.cloned.1.call-done, f32[704]{0:T(1024)S(1)} %dynamic_slice.18, ...), kind=kOutput, calls=%fused_computation | convolution fusion | flops 5913444352 | bytes 17044992 | tf_op jit(solution)/shard_map/dot_general | solution.py:40
  249.7 0.0 copy-start.3
  249.7 0.0 reduce-scatter.2.cloned.1.call-update
  249.7 0.7 copy-done.3
  250.3 11.9 %all-gather = f32[4,1,512]{2,1,0:T(1,128)S(1)} all-gather(f32[1,1,512]{2,1,0:T(1,128)S(1)} %bitcast.8), channel_id=1, replica_groups=mesh['rep'=2,'fs'=4,'tp'=4] {'fs'}, dimensions={0}, use_global_device_ids=true | all-gather | bytes 10240 | tf_op jit(solution)/shard_map/all_gather | solution.py:38
  262.3 37.4 %reduce-scatter.2.cloned.1.call-done = bf16[128,2048]{1,0:T(8,128)(2,1)} async-done(((bf16[1024,2048]{1,0:T(8,128)(2,1)}), bf16[128,2048]{1,0:T(8,128)(2,1)}) %reduce-scatter.2.cloned.1.call-update) | async-done | bytes 524304 | tf_op jit(solution)/shard_map/reduce_scatter | solution.py:39
  299.7 1.9 multiply_convert_fusion.1
  (1 shorter events, 0.0 us)
Async XLA Ops:
  6.5 1.8 copy-start
  6.5 4.4 %copy-start.1 = (bf16[128,2048]{1,0:T(8,128)(2,1)S(1)}, bf16[128,2048]{1,0:T(8,128)(2,1)}, u32[]{:S(2)}) copy-start(bf16[128,2048]{1,0:T(8,128)(2,1)} %param.8) | copy-start | bytes 1572868
  6.5 4.4 %copy-start.2 = (f32[2048]{0:T(1024)S(1)}, f32[2048]{0:T(1024)}, u32[]{:S(2)}) copy-start(f32[2048]{0:T(1024)} %param.9) | copy-start | bytes 24580
  6.5 69.4 %all-gather.8.cloned.1.call-start = ((), (), s32[]{:S(2)}) async-start(), calls=%async_computation.2 | async-start | bytes 3932160 | tf_op jit(solution)/shard_map/all_gather | solution.py:28
  9.6 103.5 %all-gather.6.cloned.1.call-start = ((), (), s32[]{:S(2)}) async-start(), calls=%async_computation.1 | async-start | bytes 4718592 | tf_op jit(solution)/shard_map/all_gather | solution.py:22
  10.9 6.3 %copy-start.4 = (f32[1408]{0:T(1024)S(1)}, f32[1408]{0:T(1024)}, u32[]{:S(2)}) copy-start(f32[1408]{0:T(1024)} %param.11) | copy-start | bytes 16900
  10.9 6.4 %copy-start.5 = (f32[1408]{0:T(1024)S(1)}, f32[1408]{0:T(1024)}, u32[]{:S(2)}) copy-start(f32[1408]{0:T(1024)} %param.13) | copy-start | bytes 16900
  11.9 166.2 %all-gather.10.cloned.1.call-start = ((), (), s32[]{:S(2)}) async-start(), calls=%async_computation.3 | async-start | bytes 3932160 | tf_op jit(solution)/shard_map/all_gather | solution.py:32
  14.8 222.6 %all-gather.12.cloned.1.call-start = ((), (), s32[]{:S(2)}) async-start(), calls=%async_computation.4 | async-start | bytes 3604480 | tf_op jit(solution)/shard_map/all_gather | solution.py:34
  17.2 282.5 %reduce-scatter.2.cloned.1.call-start = ((), (), s32[]{:S(2)}) async-start(), calls=%async_computation.5 | async-start | bytes 4718592 | tf_op jit(solution)/shard_map/reduce_scatter | solution.py:39
  249.7 0.7 copy-start.3
Sparse Core Ops, SparseCore 0:
  9.7 66.1 all-gather.7
  77.8 35.2 all-gather.5
  114.7 63.4 all-gather.9
  179.6 57.7 all-gather.11
  249.8 49.8 reduce-scatter.1
where the time goes:
time: 308 us
  waiting for transfers between devices  250 us (81%)
  matrix products  20.2 us (7%)
  between operations  13.2 us (4%)
  blocking collectives  11.9 us (4%)
  local copies, waits for them, and re-layouts  8.92 us (3%)
  other arithmetic  4.16 us (1%)
    all_gather x1, waiting for transfers between devices, shards(): down_full = lax.all_gather(down_low, 'fs', axis=1, tiled=True)  59.2 us
    all_gather x1, waiting for transfers between devices, shards(): lax.all_gather(gate_low, 'fs', axis=0, tiled=True)  58.6 us
    all_gather x1, waiting for transfers between devices, shards(): lax.all_gather(up_low, 'fs', axis=0, tiled=True)  57.1 us
    reduce_scatter x1, waiting for transfers between devices, shards(): lax.psum_scatter(jnp.dot(hidden, down_full, preferred_element_type=jnp.fl...  37.4 us
    all_gather x1, waiting for transfers between devices, shards(): group = lax.all_gather(normed, ('rep', 'tp'), axis=0, tiled=True)  37.1 us
    dot_general x1, matrix products, shards(): jnp.dot(hidden, down_full, preferred_element_type=jnp.float32)  12.3 us
    all_gather x1, blocking collectives, shards(): scales = lax.all_gather(down_scale, 'fs', axis=0, tiled=True)  11.9 us
    dot_general x1, matrix products, shards(): jnp.dot(group, lax.all_gather(gate_low, 'fs', axis=0, tiled=True), prefer...  7.9 us
  transfers between devices with their start and end apart: 5, of which 5 were waited for; matrix products, arithmetic and copies ran while one was open for 5% of the time, Pallas kernels for 0%

commit v1 on v0

--- a/solution.py
+++ b/solution.py
@@ -19,7 +19,11 @@
     mean_square = jnp.mean(flat * flat, axis=-1, keepdims=True)
     inverse = lax.rsqrt(mean_square + 1e-06)
     normed = (flat * inverse * norm_gain).astype(jnp.bfloat16)
-    group = lax.all_gather(normed, ("rep", "tp"), axis=0, tiled=True)
+    size = lax.axis_size(("rep", "tp"))
+    repeats = [size if d == 0 else 1 for d in range(normed.ndim)]
+    group = lax.all_to_all(
+        jnp.tile(normed, repeats), ("rep", "tp"), split_axis=0, concat_axis=0, tiled=True
+    )
     gate_low = part(gate_weight, 1).astype(jnp.bfloat16)
     up_low = part(up_weight, 1).astype(jnp.bfloat16)
     down_low = part(down_weight, 0).astype(jnp.bfloat16)

time: 308 us -> 270 us (0.88)
  waiting for transfers between devices: 250 us -> 205 us
  starting transfers between devices: 0.17 us -> 5.37 us
    all_gather x1, waiting for transfers between devices: 58.6 us -> 7.06 us  [shards(): lax.all_gather(gate_low, 'fs', axis=0, tiled=True)]
    all_to_all x0 -> x1, waiting for transfers between devices: none -> 45.6 us  [shards(): lax.all_to_all(jnp.tile(normed, repeats), ('rep', 'tp'), split_axis=0, co...]
    all_gather x1 -> x0, waiting for transfers between devices: 37.1 us -> none  [shards(): group = lax.all_gather(normed, ('rep', 'tp'), axis=0, tiled=True)]
    all_to_all x0 -> x1, starting transfers between devices: none -> 5.25 us  [shards(): lax.all_to_all(jnp.tile(normed, repeats), ('rep', 'tp'), split_axis=0, co...]
  transfers between devices with their start and end apart: 5 -> 5, of which waited for: 5 -> 5; matrix products, arithmetic and copies ran while one was open for 5% -> 6% of each run, Pallas kernels for 0% -> 0%
where the time goes in v1:
time: 270 us
  waiting for transfers between devices  205 us (76%)
  matrix products  20.3 us (8%)
  between operations  13.2 us (5%)
  blocking collectives  11.9 us (4%)
  local copies, waits for them, and re-layouts  11.5 us (4%)
  starting transfers between devices  5.37 us (2%)
    all_gather x1, waiting for transfers between devices, shards(): down_full = lax.all_gather(down_low, 'fs', axis=1, tiled=True)  59.4 us
    all_gather x1, waiting for transfers between devices, shards(): lax.all_gather(up_low, 'fs', axis=0, tiled=True)  55.8 us
    all_to_all x1, waiting for transfers between devices, shards(): lax.all_to_all(jnp.tile(normed, repeats), ('rep', 'tp'), split_axis=0, co...  45.6 us
    reduce_scatter x1, waiting for transfers between devices, shards(): lax.psum_scatter(jnp.dot(hidden, down_full, preferred_element_type=jnp.fl...  37.4 us
    dot_general x1, matrix products, shards(): jnp.dot(hidden, down_full, preferred_element_type=jnp.float32)  12.3 us
    all_gather x1, blocking collectives, shards(): scales = lax.all_gather(down_scale, 'fs', axis=0, tiled=True)  11.9 us
    dot_general x1, matrix products, shards(): jnp.dot(group, lax.all_gather(gate_low, 'fs', axis=0, tiled=True), prefer...  7.93 us
    all_gather x1, waiting for transfers between devices, shards(): lax.all_gather(gate_low, 'fs', axis=0, tiled=True)  7.06 us
  transfers between devices with their start and end apart: 5, of which 5 were waited for; matrix products, arithmetic and copies ran while one was open for 6% of the time, Pallas kernels for 0%

profile of v1, /device:TPU:0, one launch (start us, length us, event | category | flops | bytes accessed | tf_op | source)
XLA Modules:
  0.0 269.8 jit_solution(11367498532129998332)
XLA Ops:
  6.5 0.0 copy-start
  6.5 0.0 copy-start.1
  6.5 0.0 copy-start.2
  6.5 0.0 all-gather.5.cloned.1.call-start
  6.6 1.8 copy-done
  8.4 1.3 dynamic-slice_convert_fusion.1
  9.6 0.0 all-gather.5.cloned.1.call-update
  9.6 0.0 all-gather.7.cloned.1.call-start
  9.7 2.7 %dynamic-slice_convert_fusion = bf16[512,704]{1,0:T(8,128)(2,1)} fusion(f32[512,1408]{1,0:T(8,128)} %param.12, s32[]{:T(128)S(6)} %select_n.2), kind=kLoop, calls=%fused_computation.2 | loop fusion | bytes 1441796 | tf_op jit(solution)/shard_map/convert_element_type | solution.py:28
  12.4 0.0 all-gather.7.cloned.1.call-update
  12.4 0.0 copy-done.1
  12.4 0.2 fusion
  12.6 0.0 copy-done.2
  12.7 0.2 fusion.2
  12.9 2.5 tile.2
  15.3 0.0 copy-start.4
  15.4 0.0 copy-start.5
  15.4 5.2 %all-to-all-start = ((bf16[8,128,2048]{2,1,0:T(8,128)(2,1)}), bf16[8,128,2048]{2,1,0:T(8,128)(2,1)}, u32[]{:S(2)}, u32[]{:S(2)}) async-start(bf16[8,128,2048]{2,1,0:T(8,128)(2,1)} %tile.2), calls=%async_computation | async-start | bytes 8388608 | tf_op jit(solution)/shard_map/all_to_all | solution.py:24
  20.6 0.0 all-gather.9.cloned.1.call-start
  20.6 2.4 dynamic-slice_convert_fusion.2
  23.1 0.0 all-gather.9.cloned.1.call-update
  23.1 0.0 reduce-scatter.2.cloned.1.call-start
  23.1 0.0 copy-done.4
  23.1 0.1 dynamic_slice.16
  23.2 0.0 copy-done.5
  23.2 0.1 dynamic_slice.18
  23.3 45.6 %all-to-all-done = bf16[8,128,2048]{2,1,0:T(8,128)(2,1)} async-done(((bf16[8,128,2048]{2,1,0:T(8,128)(2,1)}), bf16[8,128,2048]{2,1,0:T(8,128)(2,1)}, u32[]{:S(2)}, u32[]{:S(2)}) %all-to-all-start) | async-done | bytes 4194336 | tf_op jit(solution)/shard_map/all_to_all | solution.py:24
  68.9 7.1 %all-gather.5.cloned.1.call-done = bf16[2048,704]{1,0:T(8,128)(2,1)} async-done(((bf16[512,704]{1,0:T(8,128)(2,1)}), bf16[2048,704]{1,0:T(8,128)(2,1)}) %all-gather.5.cloned.1.call-update) | async-done | bytes 2883600 | tf_op jit(solution)/shard_map/all_gather | solution.py:32
  76.0 7.9 %fusion.4 = f32[1024,704]{0,1:T(8,128)} fusion(bf16[1024,2048]{1,0:T(8,128)(2,1)} %bitcast, bf16[2048,704]{1,0:T(8,128)(2,1)} %all-gather.5.cloned.1.call-done), kind=kOutput, calls=%fused_computation.13 | convolution fusion | flops 2952790016 | bytes 9961472 | tf_op jit(solution)/shard_map/dot_general | solution.py:30
  83.9 55.8 %all-gather.7.cloned.1.call-done = bf16[2048,704]{1,0:T(8,128)(2,1)} async-done(((bf16[512,704]{1,0:T(8,128)(2,1)}), bf16[2048,704]{1,0:T(8,128)(2,1)}) %all-gather.7.cloned.1.call-update) | async-done | bytes 2883600 | tf_op jit(solution)/shard_map/all_gather | solution.py:36
  139.7 59.4 %all-gather.9.cloned.1.call-done = bf16[704,2048]{1,0:T(8,128)(2,1)} async-done(((bf16[704,512]{1,0:T(8,128)(2,1)}), bf16[704,2048]{1,0:T(8,128)(2,1)}) %all-gather.9.cloned.1.call-update) | async-done | bytes 2883600 | tf_op jit(solution)/shard_map/all_gather | solution.py:38
  199.0 12.3 %convolution_convert_fusion = bf16[1024,2048]{1,0:T(8,128)(2,1)} fusion(bf16[704,2048]{1,0:T(8,128)(2,1)} %all-gather.9.cloned.1.call-done, f32[1024,704]{0,1:T(8,128)} %fusion.4, bf16[1024,2048]{1,0:T(8,128)(2,1)} %bitcast, bf16[2048,704]{1,0:T(8,128)(2,1)} %all-gather.7.cloned.1.call-done, f32[704]{0:T(1024)S(1)} %dynamic_slice.18, f32[704]{0:T(1024)S(1)} %dynamic_slice.16), kind=kOutput, calls=%fused_computation | convolution fusion | flops 5913444352 | bytes 17044992 | tf_op jit(solution)/shard_map/dot_general | solution.py:44
  211.3 0.0 copy-start.3
  211.3 0.0 reduce-scatter.2.cloned.1.call-update
  211.4 0.7 copy-done.3
  212.0 11.9 %all-gather = f32[4,1,512]{2,1,0:T(1,128)S(1)} all-gather(f32[1,1,512]{2,1,0:T(1,128)S(1)} %bitcast.9), channel_id=1, replica_groups=mesh['rep'=2,'fs'=4,'tp'=4] {'fs'}, dimensions={0}, use_global_device_ids=true | all-gather | bytes 10240 | tf_op jit(solution)/shard_map/all_gather | solution.py:42
  224.0 37.4 %reduce-scatter.2.cloned.1.call-done = bf16[128,2048]{1,0:T(8,128)(2,1)} async-done(((bf16[1024,2048]{1,0:T(8,128)(2,1)}), bf16[128,2048]{1,0:T(8,128)(2,1)}) %reduce-scatter.2.cloned.1.call-update) | async-done | bytes 524304 | tf_op jit(solution)/shard_map/reduce_scatter | solution.py:43
  261.4 1.9 multiply_convert_fusion.1
  (1 shorter events, 0.0 us)
Async XLA Ops:
  6.5 1.8 copy-start
  6.5 5.9 %copy-start.1 = (bf16[128,2048]{1,0:T(8,128)(2,1)S(1)}, bf16[128,2048]{1,0:T(8,128)(2,1)}, u32[]{:S(2)}) copy-start(bf16[128,2048]{1,0:T(8,128)(2,1)} %param.8) | copy-start | bytes 1572868
  6.5 6.1 %copy-start.2 = (f32[2048]{0:T(1024)S(1)}, f32[2048]{0:T(1024)}, u32[]{:S(2)}) copy-start(f32[2048]{0:T(1024)} %param.9) | copy-start | bytes 24580
  6.5 69.4 %all-gather.5.cloned.1.call-start = ((), (), s32[]{:S(2)}) async-start(), calls=%async_computation.2 | async-start | bytes 3932160 | tf_op jit(solution)/shard_map/all_gather | solution.py:32
  9.6 130.0 %all-gather.7.cloned.1.call-start = ((), (), s32[]{:S(2)}) async-start(), calls=%async_computation.3 | async-start | bytes 3932160 | tf_op jit(solution)/shard_map/all_gather | solution.py:36
  15.3 7.8 %copy-start.4 = (f32[1408]{0:T(1024)S(1)}, f32[1408]{0:T(1024)}, u32[]{:S(2)}) copy-start(f32[1408]{0:T(1024)} %param.11) | copy-start | bytes 16900
  15.4 7.9 %copy-start.5 = (f32[1408]{0:T(1024)S(1)}, f32[1408]{0:T(1024)}, u32[]{:S(2)}) copy-start(f32[1408]{0:T(1024)} %param.13) | copy-start | bytes 16900
  15.4 53.6 %all-to-all-start = ((bf16[8,128,2048]{2,1,0:T(8,128)(2,1)}), bf16[8,128,2048]{2,1,0:T(8,128)(2,1)}, u32[]{:S(2)}, u32[]{:S(2)}) async-start(bf16[8,128,2048]{2,1,0:T(8,128)(2,1)} %tile.2), calls=%async_computation | async-start | bytes 8388608 | tf_op jit(solution)/shard_map/all_to_all | solution.py:24
  20.6 178.4 %all-gather.9.cloned.1.call-start = ((), (), s32[]{:S(2)}) async-start(), calls=%async_computation.4 | async-start | bytes 3604480 | tf_op jit(solution)/shard_map/all_gather | solution.py:38
  23.1 238.3 %reduce-scatter.2.cloned.1.call-start = ((), (), s32[]{:S(2)}) async-start(), calls=%async_computation.5 | async-start | bytes 4718592 | tf_op jit(solution)/shard_map/reduce_scatter | solution.py:43
  211.3 0.7 copy-start.3
Sparse Core Ops, SparseCore 0:
  9.8 66.1 all-gather.4
  77.5 62.0 all-gather.6
  141.2 57.7 all-gather.8
  211.5 49.8 reduce-scatter.1
